TPU v7x, 32 devices: a whole 2x2x4 slice. The times are simulated.
32 devices in a mesh: kv: 8 (over z, y), tp: 4 (over x, core).
Axes of the slice: x: 2, y: 2, z: 4, core: 2. Of those that a mesh axis runs over, the one named last changes fastest.
Arguments:
- queries: bfloat16 [1024, 1024], P('kv', 'tp'), may hold values from -6 to 6
- keys: bfloat16 [1024, 512], P('kv', 'tp'), may hold values from -6 to 6
- values: bfloat16 [1024, 512], P('kv', 'tp'), may hold values from -6 to 6
- hidden: bfloat16 [1024, 2048], P('kv'), may hold values from -6 to 6
- log_sums: float32 [2, 1024, 16], P(None, 'kv', 'tp'), may hold values from -1 to 12
- gates: float32 [2, 1024, 16], P(None, 'kv', 'tp'), may hold values from 0.1 to 0.9
- branch_out: bfloat16 [2, 1024, 1024], P(None, 'kv', 'tp'), may hold values from -6 to 6
- cotangent: bfloat16 [1024, 1024], P('kv', 'tp'), may hold values from -6 to 6
- chosen: int32 [8, 8, 48], P(None, 'tp'), may hold values from -1 to 31, as said below
Outputs:
- grad_queries: float32 [1024, 1024], P('kv', 'tp')
- grad_keys: float32 [1024, 512], P('kv', 'tp')
- grad_values: float32 [1024, 512], P('kv', 'tp')
- grad_weight: float32 [2048, 1024], P('kv', 'tp')
Inputs may be any that keep to these rules, and one draw needn't show every extreme that they name: `chosen`: each list holds global block numbers or -1. All live entries of one list name blocks of distinct owners, owner = entry // 4, none later than the list's range; list d holds min(48, d + 1) live entries, and they come first.
All inputs are finite; a program needn't handle non-finite values.
Results may differ from a plain program's by a relative error of at most 0.0055.
Values may be sent and summed in bfloat16 or wider, within the bound.
A program may use at most 64 MiB of HBM per device.

v0:
```python
import jax
import jax.numpy as jnp
from jax import lax
from jax.sharding import PartitionSpec as P

DH = 64
BLK = 32
TOPN = 12
SUB = 4
CMP = 32


def branch_grads(query_rows, key_rows, value_rows, seen, log_rows, delta_rows, cot_rows, scale):
    wide = jnp.float32
    scores = jnp.einsum("tgre,gme->grtm", query_rows, key_rows, preferred_element_type=wide) * scale
    log_here = jnp.transpose(log_rows, (1, 2, 0))[..., None]
    delta_here = jnp.transpose(delta_rows, (1, 2, 0))[..., None]
    probs = jnp.where(seen[:, None], jnp.exp(scores - log_here), 0.0)
    probs_low = probs.astype(jnp.bfloat16)
    value_grad = jnp.einsum("grtm,tgre->gme", probs_low, cot_rows, preferred_element_type=wide)
    prob_grad = jnp.einsum("tgre,gme->grtm", cot_rows, value_rows, preferred_element_type=wide)
    score_low = (probs * (prob_grad - delta_here)).astype(jnp.bfloat16)
    query_grad = (
        jnp.einsum("grtm,gme->tgre", score_low, key_rows, preferred_element_type=wide) * scale
    )
    key_grad = (
        jnp.einsum("grtm,tgre->gme", score_low, query_rows, preferred_element_type=wide) * scale
    )
    return (query_grad, key_grad, value_grad)


def shards(queries, keys, values, hidden, log_sums, gates, branch_out, cotangent, chosen):
    wide = jnp.float32
    rows_here = queries.shape[0]
    heads = queries.shape[1] // DH
    groups = keys.shape[1] // DH
    group_heads = heads // groups
    per_block = rows_here // BLK
    per_summary = rows_here // CMP
    blocks_all = chosen.shape[0]
    nsel = chosen.shape[2]
    qrows = rows_here // SUB
    scale = DH ** (-0.5)
    grads_each = jax.vmap(branch_grads, in_axes=(0, 0, 0, 0, 0, 0, 0, None))
    place = lax.axis_index("kv")
    position = place * rows_here + jnp.arange(rows_here, dtype=jnp.int32)
    gated = gates[..., None] * cotangent.reshape(rows_here, heads, DH).astype(wide)[None]
    delta_all = jnp.sum(gated * branch_out.reshape(2, rows_here, heads, DH).astype(wide), -1)
    delta_all = delta_all.reshape(2, rows_here, groups, group_heads)
    gated_low = gated.astype(jnp.bfloat16).reshape(2, rows_here, groups, group_heads, DH)
    log_all = log_sums.reshape(2, rows_here, groups, group_heads)
    query_all = queries.reshape(rows_here, groups, group_heads, DH)
    pairs = jnp.concatenate(
        [keys.reshape(rows_here, groups, DH), values.reshape(rows_here, groups, DH)], -1
    )
    means = jnp.mean(pairs.reshape(per_summary, CMP, groups, 2 * DH).astype(wide), 1).astype(
        jnp.bfloat16
    )
    summaries = lax.all_gather(means, "kv", axis=0, tiled=True)
    summary_count = summaries.shape[0]
    sum_keys = jnp.transpose(summaries[..., :DH], (1, 0, 2))
    sum_values = jnp.transpose(summaries[..., DH:], (1, 0, 2))
    summary_end = jnp.arange(summary_count, dtype=jnp.int32) * CMP + CMP - 1
    summary_seen = (summary_end[None, :] <= position[:, None])[None]
    query_sum, key_sum, value_sum = branch_grads(
        query_all, sum_keys, sum_values, summary_seen, log_all[0], delta_all[0], gated_low[0], scale
    )
    summary_term = jnp.transpose(jnp.concatenate([key_sum, value_sum], -1), (1, 0, 2))
    listing = lax.dynamic_index_in_dim(chosen, place, 0, keepdims=False)
    live = listing >= 0
    safe = jnp.maximum(listing, 0)
    owner = safe // per_block
    group_index = jnp.arange(groups, dtype=jnp.int32)
    hits = (chosen >= 0) & (chosen // per_block == place)
    wanted = jnp.sum(jnp.where(hits, chosen % per_block, 0), -1)
    asked = jnp.any(hits, -1)
    row_target = safe[..., None] * BLK + jnp.arange(BLK, dtype=jnp.int32)
    pair_blocks = pairs.reshape(per_block, BLK, groups, 2 * DH)
    outbound = pair_blocks[wanted, :, group_index[None, :], :]
    arrived = lax.all_to_all(outbound, "kv", split_axis=0, concat_axis=0, tiled=True)
    picked = arrived[owner, group_index[:, None]]

    def by_sub(array):
        rest = array.shape[3:]
        moved = array.reshape((groups, SUB, TOPN * BLK) + rest)
        return jnp.swapaxes(moved, 0, 1)

    picked_sub = by_sub(picked)
    picked_keys = picked_sub[..., :DH]
    picked_values = picked_sub[..., DH:]
    live_rows = by_sub(jnp.broadcast_to(live[..., None], (groups, nsel, BLK)))
    key_position = by_sub(row_target)
    sub_position = position.reshape(SUB, qrows)
    block_seen = live_rows[:, :, None, :] & (
        key_position[:, :, None, :] <= sub_position[:, None, :, None]
    )
    query_sel, key_sel, value_sel = grads_each(
        query_all.reshape(SUB, qrows, groups, group_heads, DH),
        picked_keys,
        picked_values,
        block_seen,
        log_all[1].reshape(SUB, qrows, groups, group_heads),
        delta_all[1].reshape(SUB, qrows, groups, group_heads),
        gated_low[1].reshape(SUB, qrows, groups, group_heads, DH),
        scale,
    )
    query_sel = query_sel.reshape(rows_here, groups, group_heads, DH)
    key_sel = jnp.swapaxes(key_sel, 0, 1).reshape(groups, nsel, BLK, DH)
    value_sel = jnp.swapaxes(value_sel, 0, 1).reshape(groups, nsel, BLK, DH)
    slot_grads = jnp.concatenate([key_sel, value_sel], -1)
    slot_grads = slot_grads * live[..., None, None].astype(wide)
    outgoing = (
        jnp.zeros((blocks_all, groups, BLK, 2 * DH), wide)
        .at[owner, group_index[:, None]]
        .add(slot_grads)
    )
    summary_out = jnp.transpose(
        summary_term.reshape(blocks_all, per_summary, groups, 2 * DH), (0, 2, 1, 3)
    )
    both_out = jnp.concatenate([outgoing, summary_out], 2)
    both_in = lax.all_to_all(
        both_out.astype(jnp.bfloat16), "kv", split_axis=0, concat_axis=0, tiled=True
    ).astype(both_out.dtype)
    incoming = both_in[:, :, :BLK]
    summary_mine = jnp.transpose(jnp.sum(both_in[:, :, BLK:], 0), (1, 0, 2))
    selector = (
        (wanted[..., None] == jnp.arange(per_block, dtype=jnp.int32)) & asked[..., None]
    ).astype(wide)
    block_sums = jnp.einsum("rgb,rgkc->bkgc", selector, incoming, precision=lax.Precision.HIGHEST)
    pair_grads = (
        block_sums.reshape(rows_here, groups, 2 * DH) + jnp.repeat(summary_mine, CMP, axis=0) / CMP
    )
    grad_queries = (query_sum + query_sel).reshape(rows_here, heads * DH)
    query_low = grad_queries.astype(jnp.bfloat16)
    grad_weight = lax.psum_scatter(
        lax.dot_general(
            hidden, query_low, (((0,), (0,)), ((), ())), preferred_element_type=jnp.float32
        ),
        "kv",
        scatter_dimension=0,
        tiled=True,
    )
    grad_keys = pair_grads[..., :DH].reshape(rows_here, groups * DH)
    grad_values = pair_grads[..., DH:].reshape(rows_here, groups * DH)
    return (grad_queries, grad_keys, grad_values, grad_weight)


def solution(mesh):
    return jax.shard_map(
        shards,
        mesh=mesh,
        in_specs=(
            P("kv", "tp"),
            P("kv", "tp"),
            P("kv", "tp"),
            P("kv", None),
            P(None, "kv", "tp"),
            P(None, "kv", "tp"),
            P(None, "kv", "tp"),
            P("kv", "tp"),
            P(None, "tp", None),
        ),
        out_specs=(P("kv", "tp"), P("kv", "tp"), P("kv", "tp"), P("kv", "tp")),
        check_vma=False,
    )
```

profile of v0, /device:TPU:0, one launch (start us, length us, event | category | flops | bytes accessed | tf_op | source)
XLA Modules:
  0.0 136.0 jit_solution(15902463175480948571)
XLA Ops:
  7.2 1.0 fusion.44
  8.2 0.9 fusion.33
  9.4 0.8 concatenate.26
  10.3 0.8 concatenate.27
  11.3 1.3 gather_fusion
  12.5 7.3 %all-to-all-start = ((bf16[8,2,32,128]{3,2,1,0:T(8,128)(2,1)}), bf16[8,2,32,128]{3,2,1,0:T(8,128)(2,1)S(1)}, u32[]{:S(2)}, u32[]{:S(2)}) async-start(bf16[8,2,32,128]{3,2,1,0:T(8,128)(2,1)} %bitcast.20), calls=%async_computation | async-start | bytes 262144 | tf_op jit(solution)/shard_map/all_to_all | solution.py:80
  19.9 0.7 multiply_bitcast_fusion.1
  20.6 0.7 fusion.45
  21.3 0.7 or_select_fusion
  22.0 1.0 copy.153
  22.9 1.0 reshape_reshape.3
  24.5 26.6 %all_gather.3 = bf16[32,2,128]{2,1,0:T(2,128)(2,1)S(1)} all-gather(bf16[4,2,128]{2,1,0:T(2,128)(2,1)S(1)} %multiply_convert_fusion.1), channel_id=1, replica_groups=mesh['kv'=8,'tp'=4] {'kv'}, dimensions={0}, use_global_device_ids=true | all-gather | bytes 18432 | tf_op jit(solution)/shard_map/all_gather | solution.py:59
  52.4 1.2 gather_fusion.1
  53.6 0.4 copy.159
  54.0 0.3 fusion.5
  54.9 0.3 copy-done.1
  55.5 1.8 %convolution_bitcast_fusion = f32[2048,256]{0,1:T(8,128)} fusion(bf16[128,2048]{1,0:T(8,128)(2,1)S(1)} %copy-done, f32[128,256]{0,1:T(8,128)S(1)} %bitcast.188), kind=kOutput, calls=%fused_computation.3 | convolution fusion | flops 134250496 | bytes 2752512 | tf_op jit(solution)/shard_map/dot_general | solution.py:136
  57.8 0.4 copy-done.3
  58.2 0.3 fusion.7
  58.5 0.5 copy.170
  59.0 1.4 %convolution_bitcast_fusion.1 = f32[2,4,384,64]{2,3,0,1:T(8,128)S(1)} fusion(f32[4,2,2,32,384]{4,3,2,1,0:T(8,128)} %copy-done.1, bf16[4,32,2,2,64]{4,1,0,3,2:T(8,128)(2,1)S(1)} %bitcast.187), kind=kOutput, calls=%fused_computation.5 | convolution fusion | flops 25362432 | bytes 1638400 | tf_op jit(solution)/shard_map/vmap(grtm,tgre->gme)/dot_general | solution.py:20
  60.4 1.6 %copy.172 = f32[2,4,384,64]{3,2,1,0:T(8,128)} copy(f32[2,4,384,64]{2,3,0,1:T(8,128)S(1)} %convolution_bitcast_fusion.1) | data formatting | bytes 1572864 | tf_op jit(solution)/shard_map/transpose | solution.py:109
  62.1 3.2 %maximum_multiply_fusion = f32[2,48,32,128]{3,2,1,0:T(8,128)} fusion(f32[2,48,32,64]{3,2,1,0:T(8,128)} %bitcast.180, f32[2,48,32,64]{3,2,1,0:T(8,128)S(1)} %bitcast.178, f32[2,48]{1,0:T(2,128)S(1)} %get-tuple-element.30), kind=kLoop, calls=%fused_computation.4 | loop fusion | flops 786432 | bytes 3146112 | tf_op jit(solution)/shard_map/mul | solution.py:111
  65.3 9.7 %scatter_fusion = f32[8,2,32,128]{3,2,1,0:T(8,128)S(1)} fusion(f32[8,2,32,128]{3,2,1,0:T(8,128)S(1)} %broadcast_in_dim.39, s32[96]{0:T(128)S(1)} %reshape.261, f32[96,32,128]{2,1,0:T(8,128)} %bitcast.179), kind=kCustom, calls=%fused_computation.2 | custom fusion | flops 393216 | bytes 4719360 | tf_op jit(solution)/shard_map/scatter-add | solution.py:115
  75.1 0.8 copy.174
  75.9 3.9 %all-to-all-start.1 = ((bf16[8,2,36,128]{3,1,2,0:T(2,128)(2,1)}), bf16[8,2,36,128]{3,1,2,0:T(2,128)(2,1)S(1)}, u32[]{:S(2)}, u32[]{:S(2)}) async-start(bf16[8,2,36,128]{3,1,2,0:T(2,128)(2,1)} %copy.174), calls=%async_computation.1 | async-start | bytes 294912 | tf_op jit(solution)/shard_map/all_to_all | solution.py:121
  79.9 0.8 copy.182
  80.6 8.5 %all-to-all-done.1 = bf16[8,2,36,128]{3,1,2,0:T(2,128)(2,1)S(1)} async-done(((bf16[8,2,36,128]{3,1,2,0:T(2,128)(2,1)}), bf16[8,2,36,128]{3,1,2,0:T(2,128)(2,1)S(1)}, u32[]{:S(2)}, u32[]{:S(2)}) %all-to-all-start.1) | async-done | bytes 147488 | tf_op jit(solution)/shard_map/all_to_all | solution.py:121
  89.8 0.7 copy.184
  90.6 0.7 copy.183
  91.3 36.1 %reduce-scatter.2.cloned.1.call-done = f32[256,256]{0,1:T(8,128)} async-done(((f32[2048,256]{0,1:T(8,128)}), f32[256,256]{0,1:T(8,128)}) %reduce-scatter.2.cloned.1.call-update) | async-done | bytes 262160 | tf_op jit(solution)/shard_map/reduce_scatter | solution.py:135
  127.4 1.8 %copy.185 = f32[256,256]{1,0:T(8,128)} copy(f32[256,256]{0,1:T(8,128)} %reduce-scatter.2.cloned.1.call-done) | data formatting | bytes 524288
  (79 shorter events, 4.4 us)
Async XLA Ops:
  7.2 48.4 %copy-start = (bf16[128,2048]{1,0:T(8,128)(2,1)S(1)}, bf16[128,2048]{1,0:T(8,128)(2,1)}, u32[]{:S(2)}) copy-start(bf16[128,2048]{1,0:T(8,128)(2,1)} %param.12) | copy-start | bytes 1572868
  7.2 16.8 %copy-start.7 = (f32[2,128,4]{1,2,0:T(4,128)S(1)}, f32[2,128,4]{1,2,0:T(4,128)}, u32[]{:S(2)}) copy-start(f32[2,128,4]{1,2,0:T(4,128)} %param.13) | copy-start | bytes 12292
  7.2 44.0 %copy-start.5 = (bf16[128,256]{1,0:T(8,128)(2,1)S(1)}, bf16[128,256]{1,0:T(8,128)(2,1)}, u32[]{:S(2)}) copy-start(bf16[128,256]{1,0:T(8,128)(2,1)} %param.16) | copy-start | bytes 196612
  7.2 44.2 %copy-start.4 = (bf16[2,128,256]{2,1,0:T(8,128)(2,1)S(1)}, bf16[2,128,256]{2,1,0:T(8,128)(2,1)}, u32[]{:S(2)}) copy-start(bf16[2,128,256]{2,1,0:T(8,128)(2,1)} %param.15) | copy-start | bytes 393220
  7.2 44.3 %copy-start.6 = (f32[2,128,4]{1,2,0:T(4,128)S(1)}, f32[2,128,4]{1,2,0:T(4,128)}, u32[]{:S(2)}) copy-start(f32[2,128,4]{1,2,0:T(4,128)} %param.14) | copy-start | bytes 12292
  12.5 39.9 %all-to-all-start = ((bf16[8,2,32,128]{3,2,1,0:T(8,128)(2,1)}), bf16[8,2,32,128]{3,2,1,0:T(8,128)(2,1)S(1)}, u32[]{:S(2)}, u32[]{:S(2)}) async-start(bf16[8,2,32,128]{3,2,1,0:T(8,128)(2,1)} %bitcast.20), calls=%async_computation | async-start | bytes 262144 | tf_op jit(solution)/shard_map/all_to_all | solution.py:80
  19.8 107.6 %reduce-scatter.2.cloned.1.call-start = ((), (), s32[]{:S(2)}) async-start(), calls=%async_computation.3 | async-start | bytes 2359296 | tf_op jit(solution)/shard_map/reduce_scatter | solution.py:135
  23.9 30.1 %copy-start.2 = (bf16[4,32,2,2,64]{4,3,2,1,0:T(2,128)(2,1)}, bf16[4,32,2,2,64]{4,3,2,1,0:T(2,128)(2,1)S(1)}, u32[]{:S(2)}) copy-start(bf16[4,32,2,2,64]{4,3,2,1,0:T(2,128)(2,1)S(1)} %reshape_reshape.3) | copy-start | bytes 196612
  54.3 0.9 copy-start.1
  57.3 0.9 copy-start.3
  75.9 13.3 %all-to-all-start.1 = ((bf16[8,2,36,128]{3,1,2,0:T(2,128)(2,1)}), bf16[8,2,36,128]{3,1,2,0:T(2,128)(2,1)S(1)}, u32[]{:S(2)}, u32[]{:S(2)}) async-start(bf16[8,2,36,128]{3,1,2,0:T(2,128)(2,1)} %copy.174), calls=%async_computation.1 | async-start | bytes 294912 | tf_op jit(solution)/shard_map/all_to_all | solution.py:121
Sparse Core Ops, SparseCore 0:
  57.4 69.8 reduce-scatter.1
where the time goes:
time: 137 us; the launch traced here: 136 us
  waiting for transfers between devices  44.6 us (33%)
  blocking collectives  26.6 us (19%)
  other arithmetic  17.5 us (13%)
  local copies, waits for them, and re-layouts  16.2 us (12%)
  between operations  14.5 us (11%)
  starting transfers between devices  11.3 us (8%)
  matrix products  5.35 us (4%)
    reduce_scatter x1, waiting for transfers between devices, shards(): lax.psum_scatter(lax.dot_general(hidden, query_low, (((0,), (0,)), ((), (...  36.1 us
    all_gather x1, blocking collectives, shards(): summaries = lax.all_gather(means, 'kv', axis=0, tiled=True)  26.6 us
    scatter-add x1, other arithmetic, shards(): outgoing = jnp.zeros((blocks_all, groups, BLK, 2 * DH), wide).at[owner, g...  9.74 us
    all_to_all x1, waiting for transfers between devices, shards(): lax.all_to_all(both_out.astype(jnp.bfloat16), 'kv', split_axis=0, concat_...  8.53 us
    all_to_all x1, starting transfers between devices, shards(): lax.all_to_all(outbound, 'kv', split_axis=0, concat_axis=0, tiled=True)  7.31 us
    unnamed x23, local copies, waits for them, and re-layouts  5.95 us
    all_to_all x1, starting transfers between devices, shards(): lax.all_to_all(both_out.astype(jnp.bfloat16), 'kv', split_axis=0, concat_...  3.92 us
    mul x1, other arithmetic, shards(): slot_grads = slot_grads * live[..., None, None].astype(wide)  3.19 us
  transfers between devices with their start and end apart: 3, of which 2 were waited for; matrix products, arithmetic and copies ran while one was open for 20% of the time, Pallas kernels for 0%

commit v1 on v0

--- a/solution.py
+++ b/solution.py
@@ -56,7 +56,14 @@
     means = jnp.mean(pairs.reshape(per_summary, CMP, groups, 2 * DH).astype(wide), 1).astype(
         jnp.bfloat16
     )
-    summaries = lax.all_gather(means, "kv", axis=0, tiled=True)
+    peers = lax.axis_size("kv")
+    hops = [(i, (i + 1) % peers) for i in range(peers)]
+    shards_2 = [means]
+    for far in range(1, peers):
+        shards_2 = [lax.ppermute(shards_2[0], "kv", hops), *shards_2]
+    whole = jnp.concatenate(shards_2, axis=0)
+    turn = (lax.axis_index("kv") + 1) * shards_2[-1].shape[0]
+    summaries = jnp.roll(whole, turn, axis=0)
     summary_count = summaries.shape[0]
     sum_keys = jnp.transpose(summaries[..., :DH], (1, 0, 2))
     sum_values = jnp.transpose(summaries[..., DH:], (1, 0, 2))

time: 137 us -> 144 us (1.051)
  waiting for transfers between devices: 44.6 us -> 77.1 us
  blocking collectives: 26.6 us -> 0 us
  starting transfers between devices: 11.3 us -> 13.4 us
    ppermute x0 -> x7, waiting for transfers between devices: none -> 34.2 us  [shards(): shards_2 = [lax.ppermute(shards_2[0], 'kv', hops), *shards_2]]
    all_gather x1 -> x0, blocking collectives: 26.6 us -> none  [shards(): summaries = lax.all_gather(means, 'kv', axis=0, tiled=True)]
    ppermute x0 -> x7, starting transfers between devices: none -> 5.09 us  [shards(): shards_2 = [lax.ppermute(shards_2[0], 'kv', hops), *shards_2]]
    all_to_all x1, starting transfers between devices: 7.31 us -> 4.88 us  [shards(): lax.all_to_all(outbound, 'kv', split_axis=0, concat_axis=0, tiled=True)]
    unnamed x23 -> x25, local copies, waits for them, and re-layouts: 5.95 us -> 5.52 us
  transfers between devices with their start and end apart: 3 -> 10, of which waited for: 2 -> 8; matrix products, arithmetic and copies ran while one was open for 20% -> 21% of each run, Pallas kernels for 0% -> 0%
where the time goes in v1:
time: 144 us
  waiting for transfers between devices  77.1 us (54%)
  other arithmetic  17.4 us (12%)
  local copies, waits for them, and re-layouts  15.7 us (11%)
  between operations  14.5 us (10%)
  starting transfers between devices  13.4 us (9%)
  matrix products  5.45 us (4%)
    reduce_scatter x1, waiting for transfers between devices, shards(): lax.psum_scatter(lax.dot_general(hidden, query_low, (((0,), (0,)), ((), (...  35.4 us
    ppermute x7, waiting for transfers between devices, shards(): shards_2 = [lax.ppermute(shards_2[0], 'kv', hops), *shards_2]  34.2 us
    scatter-add x1, other arithmetic, shards(): outgoing = jnp.zeros((blocks_all, groups, BLK, 2 * DH), wide).at[owner, g...  9.74 us
    all_to_all x1, waiting for transfers between devices, shards(): lax.all_to_all(both_out.astype(jnp.bfloat16), 'kv', split_axis=0, concat_...  7.43 us
    unnamed x25, local copies, waits for them, and re-layouts  5.52 us
    ppermute x7, starting transfers between devices, shards(): shards_2 = [lax.ppermute(shards_2[0], 'kv', hops), *shards_2]  5.09 us
    all_to_all x1, starting transfers between devices, shards(): lax.all_to_all(outbound, 'kv', split_axis=0, concat_axis=0, tiled=True)  4.88 us
    all_to_all x1, starting transfers between devices, shards(): lax.all_to_all(both_out.astype(jnp.bfloat16), 'kv', split_axis=0, concat_...  3.38 us
  transfers between devices with their start and end apart: 10, of which 8 were waited for; matrix products, arithmetic and copies ran while one was open for 21% of the time, Pallas kernels for 0%

profile of v1, /device:TPU:0, one launch (start us, length us, event | category | flops | bytes accessed | tf_op | source)
XLA Modules:
  0.0 143.6 jit_solution(10500187953345225336)
XLA Ops:
  7.2 0.9 concatenate.32
  8.2 0.8 concatenate.33
  9.1 3.0 %collective-permute-start = (bf16[4,2,128]{2,0,1:T(4,128)(2,1)S(1)}, bf16[4,2,128]{2,0,1:T(4,128)(2,1)S(1)}, u32[]{:S(2)}, u32[]{:S(2)}) collective-permute-start(bf16[4,2,128]{2,0,1:T(4,128)(2,1)S(1)} %fusion.34), channel_id=1, source_target_pairs={{0,4},{4,8},{8,12},{12,16},{16,20},{20,24},{24,28},{28,0},{1,5},{5... | collective-permute-start | bytes 6152 | tf_op jit(solution)/shard_map/ppermute | solution.py:63
  12.2 0.9 fusion.48
  13.1 0.9 fusion.33
  14.3 1.3 gather_fusion
  15.6 4.9 %all-to-all-start = ((bf16[8,2,32,128]{3,2,1,0:T(8,128)(2,1)}), bf16[8,2,32,128]{3,2,1,0:T(8,128)(2,1)S(1)}, u32[]{:S(2)}, u32[]{:S(2)}) async-start(bf16[8,2,32,128]{3,2,1,0:T(8,128)(2,1)} %bitcast.20), calls=%async_computation | async-start | bytes 262144 | tf_op jit(solution)/shard_map/all_to_all | solution.py:87
  20.5 0.7 multiply_bitcast_fusion.1
  21.2 0.7 fusion.49
  22.3 1.0 copy.152
  23.7 2.0 %collective-permute-start.1 = (bf16[4,2,128]{2,0,1:T(4,128)(2,1)S(1)}, bf16[4,2,128]{2,0,1:T(4,128)(2,1)S(1)}, u32[]{:S(2)}, u32[]{:S(2)}) collective-permute-start(bf16[4,2,128]{2,0,1:T(4,128)(2,1)S(1)} %collective-permute-done), channel_id=1, source_target_pairs={{0,4},{4,8},{8,12},{12,16},{16,20},{20,24},{24,28},{28,0},{1,5},{5... | collective-permute-start | bytes 6152 | tf_op jit(solution)/shard_map/ppermute | solution.py:63
  25.7 4.3 %collective-permute-done.1 = bf16[4,2,128]{2,0,1:T(4,128)(2,1)S(1)} collective-permute-done((bf16[4,2,128]{2,0,1:T(4,128)(2,1)S(1)}, bf16[4,2,128]{2,0,1:T(4,128)(2,1)S(1)}, u32[]{:S(2)}, u32[]{:S(2)}) %collective-permute-start.1) | collective-permute-done | bytes 2080 | tf_op jit(solution)/shard_map/ppermute | solution.py:63
  30.1 6.3 %collective-permute-done.2 = bf16[4,2,128]{2,0,1:T(4,128)(2,1)S(1)} collective-permute-done((bf16[4,2,128]{2,0,1:T(4,128)(2,1)S(1)}, bf16[4,2,128]{2,0,1:T(4,128)(2,1)S(1)}, u32[]{:S(2)}, u32[]{:S(2)}) %collective-permute-start.2) | collective-permute-done | bytes 2080 | tf_op jit(solution)/shard_map/ppermute | solution.py:63
  36.3 6.3 %collective-permute-done.3 = bf16[4,2,128]{2,0,1:T(4,128)(2,1)S(1)} collective-permute-done((bf16[4,2,128]{2,0,1:T(4,128)(2,1)S(1)}, bf16[4,2,128]{2,0,1:T(4,128)(2,1)S(1)}, u32[]{:S(2)}, u32[]{:S(2)}) %collective-permute-start.3) | collective-permute-done | bytes 2080 | tf_op jit(solution)/shard_map/ppermute | solution.py:63
  42.7 6.2 %collective-permute-done.4 = bf16[4,2,128]{2,0,1:T(4,128)(2,1)S(1)} collective-permute-done((bf16[4,2,128]{2,0,1:T(4,128)(2,1)S(1)}, bf16[4,2,128]{2,0,1:T(4,128)(2,1)S(1)}, u32[]{:S(2)}, u32[]{:S(2)}) %collective-permute-start.4) | collective-permute-done | bytes 2080 | tf_op jit(solution)/shard_map/ppermute | solution.py:63
  48.9 0.7 or_select_fusion
  49.6 5.6 %collective-permute-done.5 = bf16[4,2,128]{2,0,1:T(4,128)(2,1)S(1)} collective-permute-done((bf16[4,2,128]{2,0,1:T(4,128)(2,1)S(1)}, bf16[4,2,128]{2,0,1:T(4,128)(2,1)S(1)}, u32[]{:S(2)}, u32[]{:S(2)}) %collective-permute-start.5) | collective-permute-done | bytes 2080 | tf_op jit(solution)/shard_map/ppermute | solution.py:63
  55.9 5.6 %collective-permute-done.6 = bf16[4,2,128]{2,0,1:T(4,128)(2,1)S(1)} collective-permute-done((bf16[4,2,128]{2,0,1:T(4,128)(2,1)S(1)}, bf16[4,2,128]{2,0,1:T(4,128)(2,1)S(1)}, u32[]{:S(2)}, u32[]{:S(2)}) %collective-permute-start.6) | collective-permute-done | bytes 2080 | tf_op jit(solution)/shard_map/ppermute | solution.py:63
  62.1 1.2 gather_fusion.1
  65.2 1.8 %convolution_bitcast_fusion = f32[2048,256]{0,1:T(8,128)} fusion(bf16[128,2048]{1,0:T(8,128)(2,1)S(1)} %copy-done, f32[128,256]{0,1:T(8,128)S(1)} %bitcast.188), kind=kOutput, calls=%fused_computation.3 | convolution fusion | flops 134250496 | bytes 2752512 | tf_op jit(solution)/shard_map/dot_general | solution.py:143
  68.8 1.4 %convolution_bitcast_fusion.1 = f32[2,4,384,64]{2,3,0,1:T(8,128)S(1)} fusion(f32[4,2,2,32,384]{4,3,2,1,0:T(8,128)} %copy-done.1, bf16[4,32,2,2,64]{4,1,0,3,2:T(8,128)(2,1)S(1)} %bitcast.187), kind=kOutput, calls=%fused_computation.5 | convolution fusion | flops 25362432 | bytes 1638400 | tf_op jit(solution)/shard_map/vmap(grtm,tgre->gme)/dot_general | solution.py:20
  70.3 1.6 %copy.169 = f32[2,4,384,64]{3,2,1,0:T(8,128)} copy(f32[2,4,384,64]{2,3,0,1:T(8,128)S(1)} %convolution_bitcast_fusion.1) | data formatting | bytes 1572864 | tf_op jit(solution)/shard_map/transpose | solution.py:116
  71.9 3.2 %maximum_multiply_fusion = f32[2,48,32,128]{3,2,1,0:T(8,128)} fusion(f32[2,48,32,64]{3,2,1,0:T(8,128)} %bitcast.180, f32[2,48,32,64]{3,2,1,0:T(8,128)S(1)} %bitcast.178, f32[2,48]{1,0:T(2,128)S(1)} %get-tuple-element.30), kind=kLoop, calls=%fused_computation.4 | loop fusion | flops 786432 | bytes 3146112 | tf_op jit(solution)/shard_map/mul | solution.py:118
  75.1 9.7 %scatter_fusion = f32[8,2,32,128]{3,2,1,0:T(8,128)S(1)} fusion(f32[8,2,32,128]{3,2,1,0:T(8,128)S(1)} %broadcast_in_dim.39, s32[96]{0:T(128)S(1)} %reshape.261, f32[96,32,128]{2,1,0:T(8,128)} %bitcast.179), kind=kCustom, calls=%fused_computation.2 | custom fusion | flops 393216 | bytes 4719360 | tf_op jit(solution)/shard_map/scatter-add | solution.py:122
  84.9 0.8 copy.171
  85.7 3.4 %all-to-all-start.1 = ((bf16[8,2,36,128]{3,1,2,0:T(2,128)(2,1)}), bf16[8,2,36,128]{3,1,2,0:T(2,128)(2,1)S(1)}, u32[]{:S(2)}, u32[]{:S(2)}) async-start(bf16[8,2,36,128]{3,1,2,0:T(2,128)(2,1)} %copy.171), calls=%async_computation.1 | async-start | bytes 294912 | tf_op jit(solution)/shard_map/all_to_all | solution.py:128
  89.2 0.8 copy.179
  89.9 7.4 %all-to-all-done.1 = bf16[8,2,36,128]{3,1,2,0:T(2,128)(2,1)S(1)} async-done(((bf16[8,2,36,128]{3,1,2,0:T(2,128)(2,1)}), bf16[8,2,36,128]{3,1,2,0:T(2,128)(2,1)S(1)}, u32[]{:S(2)}, u32[]{:S(2)}) %all-to-all-start.1) | async-done | bytes 147488 | tf_op jit(solution)/shard_map/all_to_all | solution.py:128
  98.0 0.7 copy.181
  98.8 0.7 copy.180
  99.5 35.4 %reduce-scatter.2.cloned.1.call-done = f32[256,256]{0,1:T(8,128)} async-done(((f32[2048,256]{0,1:T(8,128)}), f32[256,256]{0,1:T(8,128)}) %reduce-scatter.2.cloned.1.call-update) | async-done | bytes 262160 | tf_op jit(solution)/shard_map/reduce_scatter | solution.py:142
  134.9 1.8 %copy.182 = f32[256,256]{1,0:T(8,128)} copy(f32[256,256]{0,1:T(8,128)} %reduce-scatter.2.cloned.1.call-done) | data formatting | bytes 524288
  (94 shorter events, 7.1 us)
Async XLA Ops:
  7.2 58.0 %copy-start = (bf16[128,2048]{1,0:T(8,128)(2,1)S(1)}, bf16[128,2048]{1,0:T(8,128)(2,1)}, u32[]{:S(2)}) copy-start(bf16[128,2048]{1,0:T(8,128)(2,1)} %param.12) | copy-start | bytes 1572868
  7.2 16.1 %copy-start.5 = (bf16[2,128,256]{2,1,0:T(8,128)(2,1)S(1)}, bf16[2,128,256]{2,1,0:T(8,128)(2,1)}, u32[]{:S(2)}) copy-start(bf16[2,128,256]{2,1,0:T(8,128)(2,1)} %param.15) | copy-start | bytes 393220
  7.2 16.3 %copy-start.7 = (f32[2,128,4]{1,2,0:T(4,128)S(1)}, f32[2,128,4]{1,2,0:T(4,128)}, u32[]{:S(2)}) copy-start(f32[2,128,4]{1,2,0:T(4,128)} %param.14) | copy-start | bytes 12292
  7.2 16.5 %copy-start.8 = (f32[2,128,4]{1,2,0:T(4,128)S(1)}, f32[2,128,4]{1,2,0:T(4,128)}, u32[]{:S(2)}) copy-start(f32[2,128,4]{1,2,0:T(4,128)} %param.13) | copy-start | bytes 12292
  7.2 48.0 %copy-start.4 = (bf16[128,256]{1,0:T(8,128)(2,1)S(1)}, bf16[128,256]{1,0:T(8,128)(2,1)}, u32[]{:S(2)}) copy-start(bf16[128,256]{1,0:T(8,128)(2,1)} %param.9) | copy-start | bytes 196612
  9.1 14.6 %collective-permute-start = (bf16[4,2,128]{2,0,1:T(4,128)(2,1)S(1)}, bf16[4,2,128]{2,0,1:T(4,128)(2,1)S(1)}, u32[]{:S(2)}, u32[]{:S(2)}) collective-permute-start(bf16[4,2,128]{2,0,1:T(4,128)(2,1)S(1)} %fusion.34), channel_id=1, source_target_pairs={{0,4},{4,8},{8,12},{12,16},{16,20},{20,24},{24,28},{28,0},{1,5},{5... | collective-permute-start | bytes 6152 | tf_op jit(solution)/shard_map/ppermute | solution.py:63
  15.6 46.5 %all-to-all-start = ((bf16[8,2,32,128]{3,2,1,0:T(8,128)(2,1)}), bf16[8,2,32,128]{3,2,1,0:T(8,128)(2,1)S(1)}, u32[]{:S(2)}, u32[]{:S(2)}) async-start(bf16[8,2,32,128]{3,2,1,0:T(8,128)(2,1)} %bitcast.20), calls=%async_computation | async-start | bytes 262144 | tf_op jit(solution)/shard_map/all_to_all | solution.py:87
  20.4 114.5 %reduce-scatter.2.cloned.1.call-start = ((), (), s32[]{:S(2)}) async-start(), calls=%async_computation.3 | async-start | bytes 2359296 | tf_op jit(solution)/shard_map/reduce_scatter | solution.py:142
  23.7 6.3 %collective-permute-start.1 = (bf16[4,2,128]{2,0,1:T(4,128)(2,1)S(1)}, bf16[4,2,128]{2,0,1:T(4,128)(2,1)S(1)}, u32[]{:S(2)}, u32[]{:S(2)}) collective-permute-start(bf16[4,2,128]{2,0,1:T(4,128)(2,1)S(1)} %collective-permute-done), channel_id=1, source_target_pairs={{0,4},{4,8},{8,12},{12,16},{16,20},{20,24},{24,28},{28,0},{1,5},{5... | collective-permute-start | bytes 6152 | tf_op jit(solution)/shard_map/ppermute | solution.py:63
  30.1 6.3 %collective-permute-start.2 = (bf16[4,2,128]{2,0,1:T(4,128)(2,1)S(1)}, bf16[4,2,128]{2,0,1:T(4,128)(2,1)S(1)}, u32[]{:S(2)}, u32[]{:S(2)}) collective-permute-start(bf16[4,2,128]{2,0,1:T(4,128)(2,1)S(1)} %collective-permute-done.1), channel_id=1, source_target_pairs={{0,4},{4,8},{8,12},{12,16},{16,20},{20,24},{24,28},{28,0},{1,5},{5... | collective-permute-start | bytes 6152 | tf_op jit(solution)/shard_map/ppermute | solution.py:63
  36.3 6.3 %collective-permute-start.3 = (bf16[4,2,128]{2,0,1:T(4,128)(2,1)S(1)}, bf16[4,2,128]{2,0,1:T(4,128)(2,1)S(1)}, u32[]{:S(2)}, u32[]{:S(2)}) collective-permute-start(bf16[4,2,128]{2,0,1:T(4,128)(2,1)S(1)} %collective-permute-done.2), channel_id=1, source_target_pairs={{0,4},{4,8},{8,12},{12,16},{16,20},{20,24},{24,28},{28,0},{1,5},{5... | collective-permute-start | bytes 6152 | tf_op jit(solution)/shard_map/ppermute | solution.py:63
  42.6 6.3 %collective-permute-start.4 = (bf16[4,2,128]{2,0,1:T(4,128)(2,1)S(1)}, bf16[4,2,128]{2,0,1:T(4,128)(2,1)S(1)}, u32[]{:S(2)}, u32[]{:S(2)}) collective-permute-start(bf16[4,2,128]{2,0,1:T(4,128)(2,1)S(1)} %collective-permute-done.3), channel_id=1, source_target_pairs={{0,4},{4,8},{8,12},{12,16},{16,20},{20,24},{24,28},{28,0},{1,5},{5... | collective-permute-start | bytes 6152 | tf_op jit(solution)/shard_map/ppermute | solution.py:63
  48.9 6.3 %collective-permute-start.5 = (bf16[4,2,128]{2,0,1:T(4,128)(2,1)S(1)}, bf16[4,2,128]{2,0,1:T(4,128)(2,1)S(1)}, u32[]{:S(2)}, u32[]{:S(2)}) collective-permute-start(bf16[4,2,128]{2,0,1:T(4,128)(2,1)S(1)} %collective-permute-done.4), channel_id=1, source_target_pairs={{0,4},{4,8},{8,12},{12,16},{16,20},{20,24},{24,28},{28,0},{1,5},{5... | collective-permute-start | bytes 6152 | tf_op jit(solution)/shard_map/ppermute | solution.py:63
  55.2 6.3 %collective-permute-start.6 = (bf16[4,2,128]{2,0,1:T(4,128)(2,1)S(1)}, bf16[4,2,128]{2,0,1:T(4,128)(2,1)S(1)}, u32[]{:S(2)}, u32[]{:S(2)}) collective-permute-start(bf16[4,2,128]{2,0,1:T(4,128)(2,1)S(1)} %collective-permute-done.5), channel_id=1, source_target_pairs={{0,4},{4,8},{8,12},{12,16},{16,20},{20,24},{24,28},{28,0},{1,5},{5... | collective-permute-start | bytes 6152 | tf_op jit(solution)/shard_map/ppermute | solution.py:63
  55.5 8.1 %copy-start.2 = (bf16[4,32,2,2,64]{4,3,2,1,0:T(2,128)(2,1)}, bf16[4,32,2,2,64]{4,3,2,1,0:T(2,128)(2,1)S(1)}, u32[]{:S(2)}) copy-start(bf16[4,32,2,2,64]{4,3,2,1,0:T(2,128)(2,1)S(1)} %reshape_reshape.3) | copy-start | bytes 196612
  63.9 0.9 copy-start.1
  66.9 1.1 copy-start.3
  75.1 9.8 %copy-start.6 = (bf16[8,4,2,128]{3,1,2,0:T(4,128)(2,1)S(1)}, bf16[8,4,2,128]{3,1,2,0:T(4,128)(2,1)}, u32[]{:S(2)}) copy-start(bf16[8,4,2,128]{3,1,2,0:T(4,128)(2,1)} %copy.208) | copy-start | bytes 49156
  85.7 11.7 %all-to-all-start.1 = ((bf16[8,2,36,128]{3,1,2,0:T(2,128)(2,1)}), bf16[8,2,36,128]{3,1,2,0:T(2,128)(2,1)S(1)}, u32[]{:S(2)}, u32[]{:S(2)}) async-start(bf16[8,2,36,128]{3,1,2,0:T(2,128)(2,1)} %copy.171), calls=%async_computation.1 | async-start | bytes 294912 | tf_op jit(solution)/shard_map/all_to_all | solution.py:128
Sparse Core Ops, SparseCore 0:
  67.1 67.8 reduce-scatter.1
